TPU v7x, 32 devices: a whole 2x2x4 slice. The times are simulated.
32 devices in a mesh: kv: 8 (over y, x, core), tp: 4 (over z).
Axes of the slice: x: 2, y: 2, z: 4, core: 2. Of those that a mesh axis runs over, the one named last changes fastest.
Arguments:
- tokens: bfloat16 [64, 4, 4096], P(None, None, ('kv', 'tp')), may hold values from -36 to 36
- lengths: int32 [64], replicated, may hold values from 1 to 4, 112 in all
- state: float32 [64, 128, 4096], P('kv', None, 'tp'), may hold values from -0.6 to 0.6
- attn_gain: float32 [4096], P('kv'), may hold values from 0.1 to 1.9
- w_query: bfloat16 [4096, 4096], P('kv', 'tp'), may hold values from -0.09375 to 0.09375
- w_key: bfloat16 [4096, 4096], P('kv', 'tp'), may hold values from -0.09375 to 0.09375
- w_value: bfloat16 [4096, 4096], P('kv', 'tp'), may hold values from -0.09375 to 0.09375
- w_beta: bfloat16 [4096, 32], replicated, may hold values from -0.09375 to 0.09375
- w_alpha: bfloat16 [4096, 32], replicated, may hold values from -0.09375 to 0.09375
- decay_rate: float32 [32], replicated, may hold values from 0.05 to 3
- decay_bias: float32 [32], replicated, may hold values from -3 to 3
- out_gain: float32 [128], replicated, may hold values from 0.1 to 1.9
- w_out: bfloat16 [4096, 4096], P('tp', 'kv'), may hold values from -0.09375 to 0.09375
- mix_gain: float32 [4096], P('kv'), may hold values from 0.1 to 1.9
- w_gate: bfloat16 [4096, 11008], P('kv', 'tp'), may hold values from -0.09375 to 0.09375
- w_up: bfloat16 [4096, 11008], P('kv', 'tp'), may hold values from -0.09375 to 0.09375
- w_down: bfloat16 [11008, 4096], P('tp', 'kv'), may hold values from -0.0546875 to 0.0546875
Outputs:
- mixed: bfloat16 [64, 4, 4096], P(None, None, ('kv', 'tp'))
- new_state: float32 [64, 128, 4096], P('kv', None, 'tp')
Inputs may be any that keep to these rules, and one draw needn't show every extreme that they name: Each sequence has 1 to 4 live tokens, the first ones of its block, and the lengths sum to 112.
All inputs are finite; a program needn't handle non-finite values.
Results may differ from a plain program's by a relative error of at most 0.015.
Values may be sent and summed in bfloat16 or wider, within the bound.
A program may use at most 64 MiB of HBM per device.

v0:
```python
import jax
import jax.numpy as jnp
from jax import lax
from jax.sharding import PartitionSpec as P

D = 4096
HEAD_DIM = 128


EPSILON = 1e-06


def unit_rows(vectors):
    return vectors * lax.rsqrt(jnp.sum(vectors * vectors, axis=-1, keepdims=True) + EPSILON)


def delta_block(queries, unit_keys, values_split, beta, log_decay, carried):
    highest = lax.Precision.HIGHEST
    seq_count, span_len, heads_here = beta.shape
    cumulative = jnp.cumsum(log_decay, axis=1)
    position = jnp.arange(span_len)
    inclusive = (position[:, None] >= position[None, :])[None, :, :, None]
    strict = (position[:, None] > position[None, :])[None, :, :, None]
    gap_matrix = cumulative[:, :, None, :] - cumulative[:, None, :, :]
    decay_matrix = jnp.where(inclusive, jnp.exp(jnp.where(inclusive, gap_matrix, 0.0)), 0.0)
    key_dots = jnp.einsum("nihd,njhd->nijh", unit_keys, unit_keys, precision=highest)
    query_dots = jnp.einsum("nihd,njhd->nijh", queries, unit_keys, precision=highest) * decay_matrix
    lower_part = jnp.where(strict, key_dots * decay_matrix * beta[:, :, None, :], 0.0)
    identity = jnp.eye(span_len, dtype=jnp.float32)
    inverse_rows = []
    for step in range(span_len):
        row_now = jnp.broadcast_to(identity[step][None, :, None], (seq_count, span_len, heads_here))
        for prior in range(step):
            row_now = row_now - lower_part[:, step, prior, :][:, None, :] * inverse_rows[prior]
        inverse_rows.append(row_now)
    inverse = jnp.stack(inverse_rows, axis=1)
    beta_value = beta[..., None] * values_split
    beta_key = (beta * jnp.exp(cumulative))[..., None] * unit_keys
    base_update = jnp.einsum("nich,nche->nihe", inverse, beta_value, precision=highest)
    key_weights = jnp.einsum("nich,nchd->nihd", inverse, beta_key, precision=highest)
    corrected = base_update - jnp.einsum("nihd,ndhe->nihe", key_weights, carried, precision=highest)
    decayed_queries = queries * jnp.exp(cumulative)[..., None]
    attended = jnp.einsum("nihd,ndhe->nihe", decayed_queries, carried, precision=highest)
    attended = attended + jnp.einsum("nijh,njhe->nihe", query_dots, corrected, precision=highest)
    block_total = cumulative[:, -1, :]
    key_tail = unit_keys * jnp.exp(block_total[:, None, :] - cumulative)[..., None]
    updated = carried * jnp.exp(block_total)[:, None, :, None]
    updated = updated + jnp.einsum("nihd,nihe->ndhe", key_tail, corrected, precision=highest)
    return (attended, updated)


def body(
    tokens,
    lengths,
    state,
    attn_gain,
    w_query,
    w_key,
    w_value,
    w_beta,
    w_alpha,
    decay_rate,
    decay_bias,
    out_gain,
    w_out,
    mix_gain,
    w_gate,
    w_up,
    w_down,
):
    kv_index = lax.axis_index("kv")
    tp_index = lax.axis_index("tp")
    kv_count = lax.axis_size("kv")
    batch_all, span_len, own_cols = tokens.shape
    row_count = batch_all * span_len
    seq_count = state.shape[0]
    local_rows = seq_count * span_len
    head_size = state.shape[1]
    heads_here = state.shape[2] // head_size
    block_width = attn_gain.shape[0]
    flat_rows = tokens.reshape(row_count, own_cols)
    live_all = (jnp.arange(span_len, dtype=jnp.int32)[None, :] < lengths[:, None]).reshape(
        row_count, 1
    )
    gathered = lax.all_gather(flat_rows, "tp", axis=1, tiled=True).astype(jnp.float32)
    squares_in = jnp.sum(gathered * gathered, axis=1)
    normed_in = (gathered * attn_gain).astype(jnp.bfloat16)
    beta_rows = lax.dynamic_slice_in_dim(w_beta, kv_index * block_width, block_width, 0)
    alpha_rows = lax.dynamic_slice_in_dim(w_alpha, kv_index * block_width, block_width, 0)
    query_part = jnp.dot(normed_in, w_query, preferred_element_type=jnp.float32)
    key_part = jnp.dot(normed_in, w_key, preferred_element_type=jnp.float32)
    value_part = jnp.dot(normed_in, w_value, preferred_element_type=jnp.float32)
    beta_part = jnp.dot(normed_in, beta_rows, preferred_element_type=jnp.float32)
    alpha_part = jnp.dot(normed_in, alpha_rows, preferred_element_type=jnp.float32)
    squares_all = lax.psum(squares_in, "kv")
    squares_own = lax.dynamic_slice_in_dim(squares_all, kv_index * local_rows, local_rows, 0)
    query_sum, key_sum, value_sum, beta_sum, alpha_sum = (
        lax.psum_scatter(
            query_part.astype(jnp.bfloat16), "kv", scatter_dimension=0, tiled=True
        ).astype(jnp.float32),
        lax.psum_scatter(
            key_part.astype(jnp.bfloat16), "kv", scatter_dimension=0, tiled=True
        ).astype(jnp.float32),
        lax.psum_scatter(
            value_part.astype(jnp.bfloat16), "kv", scatter_dimension=0, tiled=True
        ).astype(jnp.float32),
        lax.psum_scatter(
            beta_part.astype(jnp.bfloat16), "kv", scatter_dimension=0, tiled=True
        ).astype(jnp.float32),
        lax.psum_scatter(
            alpha_part.astype(jnp.bfloat16), "kv", scatter_dimension=0, tiled=True
        ).astype(jnp.float32),
    )
    row_scale = lax.rsqrt(squares_own / D + EPSILON)[:, None]
    head_start = tp_index * heads_here
    lengths_own = lax.dynamic_slice_in_dim(lengths, kv_index * seq_count, seq_count, 0)
    live_own = (jnp.arange(span_len, dtype=jnp.int32)[None, :] < lengths_own[:, None])[..., None]
    beta_heads = lax.dynamic_slice_in_dim(beta_sum, head_start, heads_here, 1) * row_scale
    alpha_heads = lax.dynamic_slice_in_dim(alpha_sum, head_start, heads_here, 1) * row_scale
    rate_here = lax.dynamic_slice_in_dim(decay_rate, head_start, heads_here, 0)
    bias_here = lax.dynamic_slice_in_dim(decay_bias, head_start, heads_here, 0)
    beta = jnp.where(
        live_own, jax.nn.sigmoid(beta_heads).reshape(seq_count, span_len, heads_here), 0.0
    )
    log_decay = -rate_here * jax.nn.softplus(alpha_heads + bias_here)
    log_decay = jnp.where(live_own, log_decay.reshape(seq_count, span_len, heads_here), 0.0)
    split_shape = (seq_count, span_len, heads_here, head_size)
    queries = unit_rows((query_sum * row_scale).reshape(split_shape)) * HEAD_DIM ** (-0.5)
    unit_keys = unit_rows((key_sum * row_scale).reshape(split_shape))
    values_split = (value_sum * row_scale).reshape(split_shape)
    carried = state.reshape(seq_count, head_size, heads_here, head_size)
    attended, updated = delta_block(queries, unit_keys, values_split, beta, log_decay, carried)
    head_out = (
        attended
        * lax.rsqrt(jnp.mean(attended * attended, axis=-1, keepdims=True) + EPSILON)
        * out_gain
    )
    head_out = head_out.astype(jnp.bfloat16).reshape(local_rows, heads_here * head_size)
    pack_rows = min((batch_all * 7 // 4 + kv_count - 1) // kv_count * kv_count, row_count)
    live_flat = live_all.reshape(row_count).astype(jnp.int32)
    slot_index = jnp.cumsum(live_flat) - 1
    picker = (
        (slot_index[None, :] == jnp.arange(pack_rows, dtype=jnp.int32)[:, None])
        & (live_flat[None, :] > 0)
    ).astype(jnp.bfloat16)
    heads_every = lax.all_gather(head_out, "kv", axis=0, tiled=True)
    packed_heads = jnp.dot(picker, heads_every, preferred_element_type=jnp.float32).astype(
        jnp.bfloat16
    )
    attn_part = jnp.dot(packed_heads, w_out, preferred_element_type=jnp.float32)
    base_rows = jnp.dot(picker, flat_rows, preferred_element_type=jnp.float32)
    attn_own = lax.psum_scatter(
        attn_part.astype(jnp.bfloat16), "tp", scatter_dimension=1, tiled=True
    ).astype(jnp.float32)
    middle = (base_rows + attn_own).astype(jnp.bfloat16)
    middle_rows = lax.all_gather(middle, "tp", axis=1, tiled=True).astype(jnp.float32)
    squares_mid = jnp.sum(middle_rows * middle_rows, axis=1)
    normed_mid = (middle_rows * mix_gain).astype(jnp.bfloat16)
    gate_part = jnp.dot(normed_mid, w_gate, preferred_element_type=jnp.float32)
    up_part = jnp.dot(normed_mid, w_up, preferred_element_type=jnp.float32)
    squares_total = lax.psum(squares_mid, "kv")
    gate_sum, up_sum = (
        lax.psum(gate_part.astype(jnp.bfloat16), "kv").astype(jnp.float32),
        lax.psum(up_part.astype(jnp.bfloat16), "kv").astype(jnp.float32),
    )
    mid_scale = lax.rsqrt(squares_total / D + EPSILON)[:, None]
    hidden = (jax.nn.silu(gate_sum * mid_scale) * (up_sum * mid_scale)).astype(jnp.bfloat16)
    down_part = jnp.dot(hidden, w_down, preferred_element_type=jnp.float32)
    down_own = lax.psum_scatter(
        down_part.astype(jnp.bfloat16), "tp", scatter_dimension=1, tiled=True
    ).astype(jnp.float32)
    result_rows = middle.astype(jnp.float32) + down_own
    result_rows = jnp.dot(
        picker.astype(jnp.float32).T,
        result_rows,
        precision=lax.Precision.HIGHEST,
        preferred_element_type=jnp.float32,
    )
    mixed = (
        jnp.where(live_all, result_rows, 0.0)
        .astype(jnp.bfloat16)
        .reshape(batch_all, span_len, own_cols)
    )
    return (mixed, updated.reshape(seq_count, head_size, heads_here * head_size))


def solution(mesh):
    return jax.shard_map(
        body,
        mesh=mesh,
        in_specs=(
            P(None, None, ("kv", "tp")),
            P(),
            P("kv", None, "tp"),
            P("kv"),
            P("kv", "tp"),
            P("kv", "tp"),
            P("kv", "tp"),
            P(),
            P(),
            P(),
            P(),
            P(),
            P("tp", "kv"),
            P("kv"),
            P("kv", "tp"),
            P("kv", "tp"),
            P("tp", "kv"),
        ),
        out_specs=(P(None, None, ("kv", "tp")), P("kv", None, "tp")),
        check_vma=False,
    )
```

profile of v0, /device:TPU:0, one launch (start us, length us, event | category | flops | bytes accessed | tf_op | source)
XLA Modules:
  0.0 369.6 jit_solution(18087534690063010372)
XLA Ops:
  7.2 14.8 %all_gather.9 = bf16[256,512]{1,0:T(8,128)(2,1)S(1)} all-gather(bf16[256,128]{1,0:T(8,128)(2,1)} %bitcast.99), channel_id=1, replica_groups=mesh['kv'=8,'tp'=4] {'tp'}, dimensions={1}, use_global_device_ids=true | all-gather | bytes 327680 | tf_op jit(solution)/shard_map/all_gather | solution.py:85
  22.1 1.6 convolution_convert_fusion.7
  23.8 1.6 convolution_convert_fusion.8
  25.5 2.5 convolution_convert_fusion.4
  28.0 2.5 convolution_convert_fusion.3
  30.6 2.5 convolution_convert_fusion.2
  33.1 0.1 fusion.13
  33.6 12.2 %psum.28 = f32[256]{0:T(256)S(1)} all-reduce(f32[256]{0:T(256)S(1)} %fusion.13), channel_id=1, replica_groups=mesh['kv'=8,'tp'=4] {'kv'}, use_global_device_ids=true, to_apply=%region_4.0 | all-reduce | flops 256 | bytes 2048 | tf_op jit(solution)/shard_map/psum | solution.py:95
  46.1 5.3 %copy.107 = f32[8,128,1024]{1,2,0:T(8,128)} copy(f32[8,128,1024]{2,1,0:T(8,128)} %param.19) | data formatting | bytes 8388608 | tf_op args[2]
  51.7 0.3 reduce-window.9
  52.2 0.7 add_bitcast_fusion
  52.9 0.5 convert_compare_fusion
  53.5 4.4 %reduce-scatter.16.cloned.1.call-done = bf16[32,32]{1,0:T(8,128)(2,1)} async-done(((bf16[256,32]{1,0:T(8,128)(2,1)}), bf16[32,32]{1,0:T(8,128)(2,1)}) %reduce-scatter.16.cloned.1.call-update) | async-done | bytes 2064 | tf_op jit(solution)/shard_map/reduce_scatter | solution.py:107
  57.9 36.5 %reduce-scatter.14.cloned.1.call-done = bf16[32,32]{1,0:T(8,128)(2,1)} async-done(((bf16[256,32]{1,0:T(8,128)(2,1)}), bf16[32,32]{1,0:T(8,128)(2,1)}) %reduce-scatter.14.cloned.1.call-update) | async-done | bytes 2064 | tf_op jit(solution)/shard_map/reduce_scatter | solution.py:110
  94.4 0.8 add_divide_fusion
  95.6 36.0 %reduce-scatter.12.cloned.1.call-done = bf16[32,1024]{1,0:T(8,128)(2,1)} async-done(((bf16[256,1024]{1,0:T(8,128)(2,1)}), bf16[32,1024]{1,0:T(8,128)(2,1)}) %reduce-scatter.12.cloned.1.call-update) | async-done | bytes 65552 | tf_op jit(solution)/shard_map/reduce_scatter | solution.py:98
  131.6 37.1 %reduce-scatter.18.cloned.1.call-done = bf16[32,1024]{1,0:T(8,128)(2,1)} async-done(((bf16[256,1024]{1,0:T(8,128)(2,1)}), bf16[32,1024]{1,0:T(8,128)(2,1)}) %reduce-scatter.18.cloned.1.call-update) | async-done | bytes 65552 | tf_op jit(solution)/shard_map/reduce_scatter | solution.py:104
  168.7 37.1 %reduce-scatter.20.cloned.1.call-done = bf16[32,1024]{1,0:T(8,128)(2,1)} async-done(((bf16[256,1024]{1,0:T(8,128)(2,1)}), bf16[32,1024]{1,0:T(8,128)(2,1)}) %reduce-scatter.20.cloned.1.call-update) | async-done | bytes 65552 | tf_op jit(solution)/shard_map/reduce_scatter | solution.py:101
  205.8 1.0 multiply_bitcast_fusion.2
  207.2 0.9 multiply_multiply_fusion.1
  208.1 0.6 fusion.6
  208.6 1.1 slice_reduce_fusion.4
  209.9 0.3 copy.120
  210.3 1.4 convolution_bitcast_fusion.5
  211.7 0.6 convolution_bitcast_fusion.4
  212.2 1.6 fusion.7
  213.9 8.6 %fusion.2 = f32[8,4,8,128]{3,1,2,0:T(4,128)S(1)} fusion(f32[8,4,8,128]{3,1,2,0:T(4,128)S(1)} %convolution_bitcast_fusion.5, f32[8,4,8,128]{3,1,2,0:T(4,128)S(1)} %convolution_bitcast_fusion.4, f32[8,128,8,128]{1,3,2,0:T(8,128)} %bitcast.86), kind=kOutput, calls=%fused_computation.12 | convolution fusion | flops 50364416 | bytes 4587520 | tf_op jit(solution)/shard_map/nihd,ndhe->nihe/dot_general | solution.py:41
  222.5 0.7 convolution_bitcast_fusion.2
  223.2 6.7 %multiply_reduce_fusion = (f32[8,4,8]{1,2,0:T(8,128)S(1)}, f32[8,4,8,128]{3,1,2,0:T(4,128)S(1)}) fusion(f32[8,4,8,128]{3,1,2,0:T(4,128)S(1)} %convolution_bitcast_fusion.2, f32[8,128,8,128]{1,3,2,0:T(8,128)S(1)} %bitcast.88, f32[8,4,8,128]{3,2,1,0:T(8,128)S(1)} %get-tuple-element.24), kind=kOutput, calls=%fused_computation.46 | convolution fusion | flops 50429696 | bytes 4588544 | tf_op jit(solution)/shard_map/nihd,ndhe->nihe/dot_general | solution.py:43
  230.1 0.1 multiply_convert_fusion.2
  230.3 9.8 %all_gather.10 = bf16[256,1024]{1,0:T(8,128)(2,1)S(1)} all-gather(bf16[32,1024]{1,0:T(8,128)(2,1)S(1)} %bitcast.96), channel_id=1, replica_groups=mesh['kv'=8,'tp'=4] {'kv'}, dimensions={0}, use_global_device_ids=true | all-gather | bytes 589824 | tf_op jit(solution)/shard_map/all_gather | solution.py:146
  240.1 2.3 fusion.1
  242.4 1.7 copy.137
  244.2 19.5 %reduce-scatter.22.cloned.1.call-done = bf16[128,112]{1,0:T(8,128)(2,1)} async-done(((bf16[512,112]{1,0:T(8,128)(2,1)}), bf16[128,112]{1,0:T(8,128)(2,1)}) %reduce-scatter.22.cloned.1.call-update) | async-done | bytes 28688
  263.7 0.9 copy.138
  264.6 1.0 fusion.9
  265.5 12.2 %all_gather.11 = bf16[112,512]{1,0:T(8,128)(2,1)S(1)} all-gather(bf16[112,128]{1,0:T(8,128)(2,1)S(1)} %fusion.9), channel_id=1, replica_groups=mesh['kv'=8,'tp'=4] {'tp'}, dimensions={1}, use_global_device_ids=true | all-gather | bytes 143360 | tf_op jit(solution)/shard_map/all_gather | solution.py:156
  277.7 2.6 convolution_convert_fusion
  280.3 1.8 convolution_convert_fusion.1
  282.3 12.1 %psum.30 = f32[112]{0:T(128)S(1)} all-reduce(f32[112]{0:T(128)S(1)} %fusion.15), channel_id=1, replica_groups=mesh['kv'=8,'tp'=4] {'kv'}, use_global_device_ids=true, to_apply=%region_16.17 | all-reduce | flops 112 | bytes 896 | tf_op jit(solution)/shard_map/psum | solution.py:161
  294.5 44.0 %all-reduce.3.cloned.1.call-done = (bf16[112,2752]{1,0:T(8,128)(2,1)}, bf16[112,2752]{1,0:T(8,128)(2,1)}) async-done(((bf16[112,2752]{1,0:T(8,128)(2,1)}, bf16[112,2752]{1,0:T(8,128)(2,1)}), (bf16[112,2752]{1,0:T(8,128)(2,1)}, bf16[112,2752]{1,0:T(8,128)(2,1)})) %all-reduce.3.cloned.1.call-update) | async-done | bytes 1232912 | tf_op jit(solution)/shard_map/psum | solution.py:164
  338.5 2.9 convolution_convert_fusion.6
  341.4 0.7 copy.139
  342.2 10.2 %bitcast_add_fusion = f32[8,128,8,128]{1,3,2,0:T(8,128)} fusion(f32[8,128,8,128]{1,3,2,0:T(8,128)} %bitcast.87, f32[8,4,8,128]{3,1,2,0:T(4,128)S(1)} %fusion.2, f32[8,8]{1,0:T(8,128)S(1)} %fusion.59, f32[8,4,8,128]{3,2,1,0:T(8,128)S(1)} %copy-done.3), kind=kOutput, calls=%fused_computation | convolution fusion | flops 52428800 | bytes 8651008 | tf_op jit(solution)/shard_map/nihd,nihe->ndhe/dot_general | solution.py:48
  352.4 5.4 %copy.133 = f32[8,128,1024]{2,1,0:T(8,128)} copy(f32[8,128,1024]{1,2,0:T(8,128)} %bitcast.89) | data formatting | bytes 8388608
  357.8 3.2 reduce-scatter.24.cloned.1.call-done
  360.9 0.9 copy.140
  361.8 0.9 fusion.8
  (96 shorter events, 3.1 us)
Async XLA Ops:
  7.2 270.6 %copy-start = (bf16[512,2752]{0,1:T(8,128)(2,1)S(1)}, bf16[512,2752]{0,1:T(8,128)(2,1)}, u32[]{:S(2)}) copy-start(bf16[512,2752]{0,1:T(8,128)(2,1)} %param.32) | copy-start | bytes 8454148
  7.2 20.8 %copy-start.6 = (f32[512]{0:T(512)S(1)}, f32[512]{0:T(512)}, u32[]{:S(2)}) copy-start(f32[512]{0:T(512)} %param.20) | copy-start | bytes 6148
  7.2 50.7 %reduce-scatter.16.cloned.1.call-start = ((), (), s32[]{:S(2)}) async-start(), calls=%async_computation.9 | async-start | bytes 73728 | tf_op jit(solution)/shard_map/reduce_scatter | solution.py:107
  23.7 70.7 %reduce-scatter.14.cloned.1.call-start = ((), (), s32[]{:S(2)}) async-start(), calls=%async_computation.8 | async-start | bytes 73728 | tf_op jit(solution)/shard_map/reduce_scatter | solution.py:110
  25.4 106.2 %reduce-scatter.12.cloned.1.call-start = ((), (), s32[]{:S(2)}) async-start(), calls=%async_computation.7 | async-start | bytes 589824 | tf_op jit(solution)/shard_map/reduce_scatter | solution.py:98
  27.9 5.4 %copy-start.11 = (s32[64]{0:T(128)S(1)}, s32[64]{0:T(128)}, u32[]{:S(2)}) copy-start(s32[64]{0:T(128)} %param.18) | copy-start | bytes 772
  27.9 17.9 %copy-start.14 = (f32[32]{0:T(128)S(1)}, f32[32]{0:T(128)}, u32[]{:S(2)}) copy-start(f32[32]{0:T(128)} %param.27) | copy-start | bytes 388
  27.9 18.0 %copy-start.15 = (f32[32]{0:T(128)S(1)}, f32[32]{0:T(128)}, u32[]{:S(2)}) copy-start(f32[32]{0:T(128)} %param.26) | copy-start | bytes 388
  28.0 140.8 %reduce-scatter.18.cloned.1.call-start = ((), (), s32[]{:S(2)}) async-start(), calls=%async_computation.10 | async-start | bytes 589824 | tf_op jit(solution)/shard_map/reduce_scatter | solution.py:104
  30.5 175.3 %reduce-scatter.20.cloned.1.call-start = ((), (), s32[]{:S(2)}) async-start(), calls=%async_computation.11 | async-start | bytes 589824 | tf_op jit(solution)/shard_map/reduce_scatter | solution.py:101
  33.1 230.6 %reduce-scatter.22.cloned.1.call-start = ((), (), s32[]{:S(2)}) async-start(), calls=%async_computation.12 | async-start | bytes 163840
  33.6 19.3 %copy-start.12 = (pred[256]{0:T(512)(128)(4,1)}, pred[256]{0:T(512)(128)(4,1)S(1)}, u32[]{:S(2)}) copy-start(pred[256]{0:T(512)(128)(4,1)S(1)} %lt.76) | copy-start | bytes 772
  95.6 114.2 %copy-start.5 = (f32[8,4,8]{1,2,0:T(8,128)}, f32[8,4,8]{1,2,0:T(8,128)S(1)}, u32[]{:S(2)}) copy-start(f32[8,4,8]{1,2,0:T(8,128)S(1)} %copy.111) | copy-start | bytes 3076
  212.2 10.9 %copy-start.1 = (f32[8,128,1024]{1,2,0:T(8,128)S(1)}, f32[8,128,1024]{1,2,0:T(8,128)}, u32[]{:S(2)}) copy-start(f32[8,128,1024]{1,2,0:T(8,128)} %copy.107) | copy-start | bytes 12582916
  222.5 7.7 %copy-start.9 = (f32[128]{0:T(128)S(1)}, f32[128]{0:T(128)}, u32[]{:S(2)}) copy-start(f32[128]{0:T(128)} %param.28) | copy-start | bytes 1540
  229.9 34.7 %copy-start.4 = (bf16[64,4,128]{2,1,0:T(4,128)(2,1)S(1)}, bf16[64,4,128]{2,1,0:T(4,128)(2,1)}, u32[]{:S(2)}) copy-start(bf16[64,4,128]{2,1,0:T(4,128)(2,1)} %param.17) | copy-start | bytes 196612
  242.4 37.9 %copy-start.7 = (f32[512]{0:T(512)S(1)}, f32[512]{0:T(512)}, u32[]{:S(2)}) copy-start(f32[512]{0:T(512)} %param.30) | copy-start | bytes 6148
  244.1 94.4 %all-reduce.3.cloned.1.call-start = ((), (), s32[]{:S(2)}) async-start(), calls=%async_computation.14 | async-start | bytes 2523136 | tf_op jit(solution)/shard_map/psum | solution.py:164
  264.6 15.7 %copy-start.2 = (bf16[512,2752]{0,1:T(8,128)(2,1)S(1)}, bf16[512,2752]{0,1:T(8,128)(2,1)}, u32[]{:S(2)}) copy-start(bf16[512,2752]{0,1:T(8,128)(2,1)} %param.31) | copy-start | bytes 8454148
  282.2 78.8 %reduce-scatter.24.cloned.1.call-start = ((), (), s32[]{:S(2)}) async-start(), calls=%async_computation.13 | async-start | bytes 163840
  338.5 3.7 copy-start.3
  352.4 9.4 %copy-start.8 = (s32[256]{0:T(256)S(1)}, s32[256]{0:T(256)}, u32[]{:S(2)}) copy-start(s32[256]{0:T(256)} %add_bitcast_fusion) | copy-start | bytes 3076
  352.4 9.4 %copy-start.10 = (pred[256]{0:T(512)(128)(4,1)S(1)}, pred[256]{0:T(512)(128)(4,1)}, u32[]{:S(2)}) copy-start(pred[256]{0:T(512)(128)(4,1)} %convert_compare_fusion) | copy-start | bytes 772
  352.4 9.4 %copy-start.13 = (pred[256]{0:T(512)(128)(4,1)S(1)}, pred[256]{0:T(512)(128)(4,1)}, u32[]{:S(2)}) copy-start(pred[256]{0:T(512)(128)(4,1)} %copy-done.12) | copy-start | bytes 772
Sparse Core Ops, SparseCore 0:
  23.8 34.0 reduce-scatter.15
  60.9 33.4 reduce-scatter.13
  97.5 34.1 reduce-scatter.11
  134.6 34.1 reduce-scatter.17
  171.6 34.1 reduce-scatter.19
  244.2 19.4 reduce-scatter.21
  282.3 56.1 all-reduce.2
  342.3 18.6 reduce-scatter.23
where the time goes:
time: 371 us; the launch traced here: 370 us
  waiting for transfers between devices  218 us (59%)
  blocking collectives  61.2 us (16%)
  matrix products  52.5 us (14%)
  local copies, waits for them, and re-layouts  17.7 us (5%)
  between operations  14.5 us (4%)
  other arithmetic  5.46 us (1%)
    psum x1, waiting for transfers between devices, body(): lax.psum(up_part.astype(jnp.bfloat16), 'kv').astype(jnp.float32)  44 us
    reduce_scatter x1, waiting for transfers between devices, body(): lax.psum_scatter(value_part.astype(jnp.bfloat16), 'kv', scatter_dimension...  37.1 us
    reduce_scatter x1, waiting for transfers between devices, body(): lax.psum_scatter(key_part.astype(jnp.bfloat16), 'kv', scatter_dimension=0...  37.1 us
    reduce_scatter x1, waiting for transfers between devices, body(): lax.psum_scatter(alpha_part.astype(jnp.bfloat16), 'kv', scatter_dimension...  36.5 us
    reduce_scatter x1, waiting for transfers between devices, body(): lax.psum_scatter(query_part.astype(jnp.bfloat16), 'kv', scatter_dimension...  36 us
    unnamed x10, waiting for transfers between devices  22.8 us
    unnamed x42, local copies, waits for them, and re-layouts  15 us
    all_gather x1, blocking collectives, body(): lax.all_gather(flat_rows, 'tp', axis=1, tiled=True).astype(jnp.float32)  14.8 us
  transfers between devices with their start and end apart: 8, of which 8 were waited for; matrix products, arithmetic and copies ran while one was open for 9% of the time, Pallas kernels for 0%

commit v1 on v0

--- a/solution.py
+++ b/solution.py
@@ -1,7 +1,13 @@
 import jax
 import jax.numpy as jnp
 from jax import lax
+from jax.experimental import pallas as pl
+from jax.experimental.pallas import tpu as pltpu
 from jax.sharding import PartitionSpec as P
+
+MESH = pl.DeviceIdType.MESH
+F32 = jnp.float32
+BF16 = jnp.bfloat16
 
 D = 4096
 HEAD_DIM = 128
@@ -184,9 +190,585 @@
     return (mixed, updated.reshape(seq_count, head_size, heads_here * head_size))
 
 
+def iota(shape, axis):
+    return lax.broadcasted_iota(jnp.int32, shape, axis)
+
+
+def dot(a, b):
+    return jnp.dot(a, b, preferred_element_type=F32)
+
+
+def dot_exact(a, b):
+    return jnp.dot(a, b, precision=lax.Precision.HIGHEST, preferred_element_type=F32)
+
+
+def head_sum(x, heads, size):
+    pieces = []
+    for h in range(heads):
+        total = jnp.sum(x[:, h * size : (h + 1) * size], axis=1, keepdims=True)
+        pieces.append(jnp.broadcast_to(total, (x.shape[0], size)))
+    return jnp.concatenate(pieces, axis=1)
+
+
+def high_low(x):
+    high = x.astype(BF16)
+    return high.astype(F32), x - high.astype(F32)
+
+
+def layer_kernel(
+    dims,
+    tokens_ref,
+    lengths_ref,
+    state_hbm,
+    attn_gain_ref,
+    wq_hbm,
+    wk_hbm,
+    wv_hbm,
+    wb_hbm,
+    wa_hbm,
+    rate_ref,
+    bias_ref,
+    out_gain_ref,
+    wo_hbm,
+    mix_gain_ref,
+    wg_hbm,
+    wu_hbm,
+    wd_hbm,
+    mixed_ref,
+    new_state_hbm,
+    state,
+    w_qkv,
+    w_beta,
+    w_alpha,
+    w_out,
+    w_gate,
+    w_up,
+    w_down,
+    tok_all,
+    qkv_part,
+    qkv_pair,
+    qkv_red,
+    qkv_recv,
+    head_all,
+    attn_part,
+    attn_recv,
+    mid_all,
+    gu_part,
+    gu_pair,
+    gu_red,
+    gu_recv,
+    hid_all,
+    down_part,
+    down_recv,
+    load_sem,
+    store_sem,
+    tp_send,
+    tp_recv,
+    pair_send,
+    pair_recv,
+    chip_send,
+    chip_recv,
+    fwd_send,
+    fwd_recv,
+):
+    n_kv, n_tp, batch, span, seqs, heads, size, width, ff, rows, unit = dims
+    chips = n_kv // 2
+    kv = lax.axis_index("kv")
+    tp = lax.axis_index("tp")
+    core = lax.rem(kv, 2)
+    chip = kv // 2
+    other = 1 - core
+    partner = chip * 2 + other
+    slots = batch * span
+    local = seqs * span
+    vw = heads * size
+
+    def chip_at(d):
+        return lax.rem(chip + d, chips)
+
+    def chip_from(d):
+        return lax.rem(chip + chips - d, chips)
+
+    loads = [
+        pltpu.make_async_copy(wq_hbm, w_qkv.at[0], load_sem.at[0]),
+        pltpu.make_async_copy(wk_hbm, w_qkv.at[1], load_sem.at[1]),
+        pltpu.make_async_copy(wv_hbm, w_qkv.at[2], load_sem.at[2]),
+        pltpu.make_async_copy(
+            wb_hbm.at[pl.ds(pl.multiple_of(kv * width, width), width), :], w_beta, load_sem.at[3]
+        ),
+        pltpu.make_async_copy(
+            wa_hbm.at[pl.ds(pl.multiple_of(kv * width, width), width), :], w_alpha, load_sem.at[4]
+        ),
+        pltpu.make_async_copy(state_hbm, state, load_sem.at[5]),
+        pltpu.make_async_copy(wo_hbm, w_out, load_sem.at[6]),
+        pltpu.make_async_copy(wg_hbm, w_gate, load_sem.at[7]),
+        pltpu.make_async_copy(wu_hbm, w_up, load_sem.at[8]),
+        pltpu.make_async_copy(wd_hbm, w_down, load_sem.at[9]),
+    ]
+    for load in loads:
+        load.start()
+
+    barrier = pltpu.get_barrier_semaphore()
+    pl.semaphore_signal(barrier, inc=1, device_id={"kv": partner}, device_id_type=MESH)
+    for d in range(1, chips):
+        pl.semaphore_signal(
+            barrier, inc=1, device_id={"kv": chip_at(d) * 2 + core}, device_id_type=MESH
+        )
+    for d in range(1, n_tp):
+        pl.semaphore_signal(
+            barrier, inc=1, device_id={"tp": lax.rem(tp + d, n_tp)}, device_id_type=MESH
+        )
+
+    lengths_row = lengths_ref[...].astype(F32)
+    spread = (iota((batch, slots), 1) // span == iota((batch, slots), 0)).astype(BF16)
+    length_of = dot(jnp.broadcast_to(lengths_row, (8, batch)).astype(BF16), spread)
+    live_row = (lax.rem(iota((8, slots), 1), span).astype(F32) < length_of).astype(F32)
+    before = (iota((slots, slots), 0) < iota((slots, slots), 1)).astype(BF16)
+    slot_row = dot(live_row.astype(BF16), before)
+    slot_row = jnp.where(live_row > 0.0, slot_row, -1.0)[0:1, :]
+    picker = (iota((rows, slots), 0).astype(F32) == slot_row).astype(BF16)
+    position = iota((slots, slots), 1) // local
+    inner = lax.rem(iota((slots, slots), 1), local)
+    from_slot = (
+        (lax.rem(position, chips) * 2 + position // chips) * seqs + lax.rem(inner, seqs)
+    ) * span + inner // seqs
+    order = (iota((slots, slots), 0) == from_slot).astype(BF16)
+    picker_kv = dot(picker, order).astype(BF16)
+
+    own_tokens = dot(picker, tokens_ref[...])
+    tok_all[tp] = own_tokens.astype(BF16)
+    pl.semaphore_wait(barrier, 1 + (chips - 1) + (n_tp - 1))
+
+    def tp_copies(phase, source_at, dest_at):
+        copies = []
+        for d in range(1, n_tp):
+            peer = lax.rem(tp + d, n_tp)
+            copies.append(
+                pltpu.make_async_remote_copy(
+                    src_ref=source_at(peer, d),
+                    dst_ref=dest_at(peer, d),
+                    send_sem=tp_send.at[phase, d - 1],
+                    recv_sem=tp_recv.at[phase, d - 1],
+                    device_id={"tp": peer},
+                    device_id_type=MESH,
+                )
+            )
+        return copies
+
+    def exchange_start(copies):
+        for copy in copies:
+            copy.start()
+
+    def exchange_wait(copies):
+        for copy in copies:
+            copy.wait()
+
+    copies = tp_copies(0, lambda peer, d: tok_all.at[tp], lambda peer, d: tok_all.at[tp])
+    exchange_start(copies)
+    exchange_wait(copies)
+    gathered = jnp.concatenate([tok_all[j] for j in range(n_tp)], axis=1).astype(F32)
+    squares = jnp.sum(gathered * gathered, axis=1, keepdims=True)
+    normed = (gathered * attn_gain_ref[...]).astype(BF16)
+    square_high, square_low = high_low(squares)
+    square_pair = jnp.concatenate([square_high, square_low], axis=1).astype(BF16)
+
+    def place(rows_packed):
+        return lax.dot_general(
+            picker_kv, rows_packed, (((0,), (0,)), ((), ())), preferred_element_type=F32
+        ).astype(BF16)
+
+    placed = place(normed)
+    square_placed = place(square_pair)
+    half = chips * local
+    n_heads_all = wb_hbm.shape[1]
+    qkv_width = 3 * vw + 128
+    for load in loads[0:5]:
+        load.wait()
+    for c in range(2):
+        here = placed[c * half : (c + 1) * half, :]
+        part = slice(c * half, (c + 1) * half)
+        for m in range(3):
+            qkv_part[part, m * vw : (m + 1) * vw] = dot(here, w_qkv[m]).astype(BF16)
+        extra = jnp.concatenate(
+            [
+                dot(here, w_beta[...]),
+                dot(here, w_alpha[...]),
+                square_placed[part, :].astype(F32),
+                jnp.zeros((half, 128 - 2 * n_heads_all - 2), F32),
+            ],
+            axis=1,
+        )
+        qkv_part[part, 3 * vw : qkv_width] = extra.astype(BF16)
+
+    pair_copy = pltpu.make_async_remote_copy(
+        src_ref=qkv_part.at[pl.ds(pl.multiple_of(other * half, half), half), :],
+        dst_ref=qkv_pair,
+        send_sem=pair_send.at[0],
+        recv_sem=pair_recv.at[0],
+        device_id={"kv": partner},
+        device_id_type=MESH,
+    )
+    pair_copy.start()
+    pair_copy.wait()
+    copies = []
+    for d in range(1, chips):
+        dest = chip_at(d)
+        at = pl.ds(pl.multiple_of(dest * local, local), local)
+        mine = pl.ds(pl.multiple_of(core * half + dest * local, local), local)
+        qkv_red[d - 1] = (qkv_part[mine, :].astype(F32) + qkv_pair[at, :].astype(F32)).astype(BF16)
+        copies.append(
+            pltpu.make_async_remote_copy(
+                src_ref=qkv_red.at[d - 1],
+                dst_ref=qkv_recv.at[d - 1],
+                send_sem=chip_send.at[0, d - 1],
+                recv_sem=chip_recv.at[0, d - 1],
+                device_id={"kv": dest * 2 + core},
+                device_id_type=MESH,
+            )
+        )
+        copies[-1].start()
+    at = pl.ds(pl.multiple_of(chip * local, local), local)
+    mine = pl.ds(pl.multiple_of(core * half + chip * local, local), local)
+    total = qkv_part[mine, :].astype(F32) + qkv_pair[at, :].astype(F32)
+
+    loads[5].wait()
+    state_low = state[...].reshape(seqs * size, vw).astype(BF16)
+    exchange_wait(copies)
+    for d in range(1, chips):
+        total = total + qkv_recv[d - 1].astype(F32)
+
+    extra = total[:, 3 * vw : qkv_width]
+    lane = iota((local, 128), 1)
+    sq_lane = (lane == 2 * n_heads_all) | (lane == 2 * n_heads_all + 1)
+    sq_own = jnp.sum(jnp.where(sq_lane, extra, 0.0), axis=1, keepdims=True)
+    row_scale = lax.rsqrt(sq_own / D + EPSILON)
+    scaled_extra = jnp.where(sq_lane, 0.0, extra * row_scale)
+    lane_of = iota((128, vw), 0)
+    head_of = iota((128, vw), 1) // size + tp * heads
+    beta_pre = dot_exact(scaled_extra, (lane_of == head_of).astype(F32))
+    alpha_pre = dot_exact(scaled_extra, (lane_of == head_of + n_heads_all).astype(F32))
+    per_head = (iota((n_heads_all, vw), 0) == iota((n_heads_all, vw), 1) // size + tp * heads).astype(F32)
+    rate = dot_exact(jnp.broadcast_to(rate_ref[...], (8, n_heads_all)), per_head)[0:1, :]
+    bias = dot_exact(jnp.broadcast_to(bias_ref[...], (8, n_heads_all)), per_head)[0:1, :]
+    row_id = iota((local, batch), 0)
+    seq_hit = iota((local, batch), 1) == kv * seqs + lax.rem(row_id, seqs)
+    own_len = jnp.sum(jnp.where(seq_hit, lengths_row, 0.0), axis=1, keepdims=True)
+    live = (iota((local, 1), 0) // seqs).astype(F32) < own_len
+    beta = jnp.where(live, 1.0 / (1.0 + jnp.exp(-beta_pre)), 0.0)
+    pre = alpha_pre + bias
+    softplus = jnp.maximum(pre, 0.0) + jnp.log(1.0 + jnp.exp(-jnp.abs(pre)))
+    log_decay = jnp.where(live, -rate * softplus, 0.0)
+
+    q_raw = total[:, 0:vw] * row_scale
+    k_raw = total[:, vw : 2 * vw] * row_scale
+    values = total[:, 2 * vw : 3 * vw] * row_scale
+    queries = q_raw * lax.rsqrt(head_sum(q_raw * q_raw, heads, size) + EPSILON) * size ** (-0.5)
+    keys = k_raw * lax.rsqrt(head_sum(k_raw * k_raw, heads, size) + EPSILON)
+
+    def token(x, t):
+        return x[t * seqs : (t + 1) * seqs, :]
+
+    cumulative = [token(log_decay, 0)]
+    for t in range(1, span):
+        cumulative.append(cumulative[-1] + token(log_decay, t))
+
+    def blocked(x):
+        keep = lax.rem(iota(x.shape, 0), seqs)
+        return jnp.concatenate(
+            [jnp.where(keep == n, x, 0.0).astype(BF16) for n in range(seqs)], axis=1
+        )
+
+    products = []
+    for h in range(heads):
+        cols = slice(h * size, (h + 1) * size)
+        both = jnp.concatenate([keys[:, cols], queries[:, cols]], axis=0)
+        products.append(dot(blocked(both), state_low[:, cols]))
+    products = jnp.concatenate(products, axis=1)
+    updates, attended = [], []
+    for t in range(span):
+        grown = jnp.exp(cumulative[t])
+        update = token(values, t) - grown * token(products, t)
+        for p in range(t):
+            weight = jnp.exp(cumulative[t] - cumulative[p]) * head_sum(
+                token(keys, t) * token(keys, p), heads, size
+            )
+            update = update - weight * updates[p]
+        updates.append(token(beta, t) * update)
+        result = grown * token(products, span + t)
+        for p in range(t + 1):
+            weight = jnp.exp(cumulative[t] - cumulative[p]) * head_sum(
+                token(queries, t) * token(keys, p), heads, size
+            )
+            result = result + weight * updates[p]
+        attended.append(result)
+    attended = jnp.concatenate(attended, axis=0)
+    gain = jnp.concatenate([out_gain_ref[...]] * heads, axis=1)
+    head_out = attended * lax.rsqrt(head_sum(attended * attended, heads, size) / size + EPSILON) * gain
+
+    def kv_gather_start(phase, buffer):
+        spot = core * chips + chip
+        own = pltpu.make_async_remote_copy(
+            src_ref=buffer.at[spot],
+            dst_ref=buffer.at[spot],
+            send_sem=fwd_send.at[phase, 0],
+            recv_sem=fwd_recv.at[phase, 0],
+            device_id={"kv": partner},
+            device_id_type=MESH,
+        )
+        far = [
+            pltpu.make_async_remote_copy(
+                src_ref=buffer.at[spot],
+                dst_ref=buffer.at[spot],
+                send_sem=chip_send.at[1 + 2 * phase, d - 1],
+                recv_sem=chip_recv.at[1 + 2 * phase, d - 1],
+                device_id={"kv": chip_at(d) * 2 + core},
+                device_id_type=MESH,
+            )
+            for d in range(1, chips)
+        ]
+        exchange_start(far)
+        own.start()
+        return own, far
+
+    def kv_gather_finish(phase, buffer, own, far):
+        forwards = []
+        for d in range(1, chips):
+            far[d - 1].wait_recv()
+            spot = core * chips + chip_from(d)
+            forwards.append(
+                pltpu.make_async_remote_copy(
+                    src_ref=buffer.at[spot],
+                    dst_ref=buffer.at[spot],
+                    send_sem=fwd_send.at[phase, d],
+                    recv_sem=fwd_recv.at[phase, d],
+                    device_id={"kv": partner},
+                    device_id_type=MESH,
+                )
+            )
+            forwards[-1].start()
+        own.wait()
+        exchange_wait(forwards)
+        for copy in far:
+            copy.wait_send()
+
+    head_all[core * chips + chip] = head_out.astype(BF16)
+    own, far = kv_gather_start(0, head_all)
+
+    final = cumulative[-1]
+    tails = jnp.concatenate(
+        [token(keys, t) * jnp.exp(final - cumulative[t]) for t in range(span)], axis=0
+    )
+    all_updates = jnp.concatenate(updates, axis=0).astype(BF16)
+    decay_all = jnp.exp(final)
+    for h in range(heads):
+        cols = slice(h * size, (h + 1) * size)
+        rank = lax.dot_general(
+            blocked(tails[:, cols]),
+            all_updates[:, cols],
+            (((0,), (0,)), ((), ())),
+            preferred_element_type=F32,
+        )
+        for n in range(seqs):
+            state[n, :, cols] = (
+                state[n, :, cols] * decay_all[n : n + 1, cols] + rank[n * size : (n + 1) * size, :]
+            )
+    write_state = pltpu.make_async_copy(state, new_state_hbm, store_sem.at[0])
+    write_state.start()
+
+    kv_gather_finish(0, head_all, own, far)
+    heads_every = head_all[...].reshape(slots, vw)
+    packed = dot(picker_kv, heads_every).astype(BF16)
+    loads[6].wait()
+    part = dot(packed, w_out[...])
+    own_cols = tokens_ref.shape[1]
+
+    def tp_scatter(phase, part, part_ref, recv_ref):
+        for j in range(n_tp):
+            part_ref[j] = part[:, j * own_cols : (j + 1) * own_cols].astype(BF16)
+        copies = tp_copies(
+            phase, lambda peer, d: part_ref.at[peer], lambda peer, d: recv_ref.at[d - 1]
+        )
+        exchange_start(copies)
+        exchange_wait(copies)
+        total = part_ref[tp].astype(F32)
+        for d in range(1, n_tp):
+            total = total + recv_ref[d - 1].astype(F32)
+        return total
+
+    middle = (own_tokens + tp_scatter(1, part, attn_part, attn_recv)).astype(BF16)
+    mid_all[tp] = middle
+    copies = tp_copies(2, lambda peer, d: mid_all.at[tp], lambda peer, d: mid_all.at[tp])
+    exchange_start(copies)
+    exchange_wait(copies)
+    middle_rows = jnp.concatenate([mid_all[j] for j in range(n_tp)], axis=1).astype(F32)
+    squares = jnp.sum(middle_rows * middle_rows, axis=1, keepdims=True)
+    normed_mid = (middle_rows * mix_gain_ref[...]).astype(BF16)
+    square_high, square_low = high_low(squares)
+    pad = gu_part.shape[2] - ff
+    side = jnp.concatenate([square_high, square_low, jnp.zeros((rows, pad - 2), F32)], axis=1)
+    half = chips * unit
+    copies = []
+    for m in range(2):
+        loads[7 + m].wait()
+        gu_part[m, :, 0:ff] = dot(normed_mid, (w_gate, w_up)[m][...]).astype(BF16)
+        gu_part[m, :, ff:] = (side if m == 0 else jnp.zeros((rows, pad), F32)).astype(BF16)
+        copies.append(
+            pltpu.make_async_remote_copy(
+                src_ref=gu_part.at[m, pl.ds(pl.multiple_of(other * half, half), half), :],
+                dst_ref=gu_pair.at[m],
+                send_sem=pair_send.at[1 + m],
+                recv_sem=pair_recv.at[1 + m],
+                device_id={"kv": partner},
+                device_id_type=MESH,
+            )
+        )
+        copies[-1].start()
+    far = []
+    for m in range(2):
+        copies[m].wait()
+        for d in range(1, chips):
+            dest = chip_at(d)
+            at = pl.ds(pl.multiple_of(dest * unit, unit), unit)
+            mine = pl.ds(pl.multiple_of(core * half + dest * unit, unit), unit)
+            gu_red[m, d - 1] = (
+                gu_part[m, mine, :].astype(F32) + gu_pair[m, at, :].astype(F32)
+            ).astype(BF16)
+            far.append(
+                pltpu.make_async_remote_copy(
+                    src_ref=gu_red.at[m, d - 1],
+                    dst_ref=gu_recv.at[m, d - 1],
+                    send_sem=chip_send.at[2 if m == 0 else 4, d - 1],
+                    recv_sem=chip_recv.at[2 if m == 0 else 4, d - 1],
+                    device_id={"kv": dest * 2 + core},
+                    device_id_type=MESH,
+                )
+            )
+            far[-1].start()
+    at = pl.ds(pl.multiple_of(chip * unit, unit), unit)
+    mine = pl.ds(pl.multiple_of(core * half + chip * unit, unit), unit)
+    sums = []
+    for m in range(2):
+        sums.append(gu_part[m, mine, :].astype(F32) + gu_pair[m, at, :].astype(F32))
+    exchange_wait(far)
+    for m in range(2):
+        for d in range(1, chips):
+            sums[m] = sums[m] + gu_recv[m, d - 1].astype(F32)
+    gate, up = sums
+    lane = iota(gate.shape, 1)
+    sq_mid = jnp.sum(
+        jnp.where((lane == ff) | (lane == ff + 1), gate, 0.0), axis=1, keepdims=True
+    )
+    mid_scale = lax.rsqrt(sq_mid / D + EPSILON)
+    gate = jnp.where(lane < ff, gate * mid_scale, 0.0)
+    hidden = gate / (1.0 + jnp.exp(-gate)) * (up * mid_scale)
+    hid_all[core * chips + chip] = hidden.astype(BF16)
+    own, far = kv_gather_start(1, hid_all)
+    kv_gather_finish(1, hid_all, own, far)
+    loads[9].wait()
+    hidden_all = hid_all[...].reshape(rows, hid_all.shape[2])[:, 0:ff]
+    part = dot(hidden_all, w_down[...])
+    result = (middle.astype(F32) + tp_scatter(3, part, down_part, down_recv)).astype(BF16)
+    mixed_ref[...] = lax.dot_general(
+        picker, result, (((0,), (0,)), ((), ())), preferred_element_type=F32
+    ).astype(BF16)
+    write_state.wait()
+
+
+def fused_layer(n_kv, n_tp, *args):
+    tokens, lengths, state, attn_gain, w_query = args[:5]
+    w_beta, w_out, w_gate = args[7], args[12], args[14]
+    batch, span, own_cols = tokens.shape
+    seqs, size, vw = state.shape
+    heads = vw // size
+    width = attn_gain.shape[0]
+    ff = w_gate.shape[1]
+    pack = min(batch * 7 // 4, batch * span)
+    unit = (pack + n_kv - 1) // n_kv
+    unit = (unit + 15) // 16 * 16
+    rows = unit * n_kv
+    local = seqs * span
+    chips = n_kv // 2
+    ff_pad = (ff + 2 + 127) // 128 * 128
+    qkv_width = 3 * vw + 128
+    dims = (n_kv, n_tp, batch, span, seqs, heads, size, width, ff, rows, unit)
+    operands = list(args)
+    operands[0] = tokens.reshape(batch * span, own_cols)
+    for at in (1, 3, 9, 10, 11, 13):
+        operands[at] = operands[at].reshape(1, -1)
+    in_vmem = pl.BlockSpec(memory_space=pltpu.VMEM)
+    in_hbm = pl.BlockSpec(memory_space=pl.ANY)
+    vmem_args = (0, 1, 3, 9, 10, 11, 13)
+    dma = pltpu.SemaphoreType.DMA
+
+    def buf(*shape):
+        return pltpu.VMEM(shape, BF16)
+
+    mixed, new_state = pl.pallas_call(
+        lambda *refs: layer_kernel(dims, *refs),
+        out_shape=(
+            jax.ShapeDtypeStruct((batch * span, own_cols), BF16),
+            jax.ShapeDtypeStruct(state.shape, F32),
+        ),
+        in_specs=[in_vmem if i in vmem_args else in_hbm for i in range(len(operands))],
+        out_specs=(in_vmem, in_hbm),
+        scratch_shapes=[
+            pltpu.VMEM(state.shape, F32),
+            buf(3, width, vw),
+            buf(*(width, w_beta.shape[1])),
+            buf(*(width, w_beta.shape[1])),
+            buf(*w_out.shape),
+            buf(*w_gate.shape),
+            buf(*w_gate.shape),
+            buf(ff, w_out.shape[1]),
+            buf(n_tp, rows, own_cols),
+            buf(n_kv * local, qkv_width),
+            buf(chips * local, qkv_width),
+            buf(chips - 1, local, qkv_width),
+            buf(chips - 1, local, qkv_width),
+            buf(n_kv, local, vw),
+            buf(n_tp, rows, own_cols),
+            buf(n_tp - 1, rows, own_cols),
+            buf(n_tp, rows, own_cols),
+            buf(2, rows, ff_pad),
+            buf(2, chips * unit, ff_pad),
+            buf(2, chips - 1, unit, ff_pad),
+            buf(2, chips - 1, unit, ff_pad),
+            buf(n_kv, unit, ff_pad),
+            buf(n_tp, rows, own_cols),
+            buf(n_tp - 1, rows, own_cols),
+            dma((10,)),
+            dma((1,)),
+            dma((4, n_tp - 1)),
+            dma((4, n_tp - 1)),
+            dma((3,)),
+            dma((3,)),
+            dma((5, chips - 1)),
+            dma((5, chips - 1)),
+            dma((2, chips)),
+            dma((2, chips)),
+        ],
+        compiler_params=pltpu.CompilerParams(
+            collective_id=0, has_side_effects=True, vmem_limit_bytes=60 * 1024 * 1024
+        ),
+    )(*operands)
+    return mixed.reshape(tokens.shape), new_state
+
+
+def layer(*args):
+    n_kv, n_tp = lax.axis_size("kv"), lax.axis_size("tp")
+    tokens, state = args[0], args[2]
+    batch, span, own_cols = tokens.shape
+    seqs, size, vw = state.shape
+    aligned = own_cols % 128 == 0 and size % 128 == 0 and seqs == 8
+    aligned = aligned and n_kv % 2 == 0 and 2 * args[7].shape[1] + 2 <= 128
+    if aligned:
+        return fused_layer(n_kv, n_tp, *args)
+    return body(*args)
+
+
 def solution(mesh):
     return jax.shard_map(
-        body,
+        layer,
         mesh=mesh,
         in_specs=(
             P(None, None, ("kv", "tp")),

time: 371 us -> 87.9 us (0.24)
  waiting for transfers between devices: 218 us -> 0 us
  Pallas kernels: 0 us -> 68.4 us
  blocking collectives: 61.2 us -> 0 us
  matrix products: 52.5 us -> 0 us
  between operations: 14.5 us -> 0.64 us
  other arithmetic: 5.46 us -> 0 us
    reduce_scatter x5 -> x0, waiting for transfers between devices: 151 us -> none  [the longest x1 37.1 us: body(): lax.psum_scatter(value_part.astype(jnp.bfloat16), 'kv', scatter_dimension...]
    pallas_call x0 -> x1, Pallas kernels: none -> 68.4 us  [fused_layer(): pl.pallas_call(lambda *refs: layer_kernel(dims, *refs), out_shape=(jax.Sh...]
    dot_general x19 -> x0, matrix products: 52.5 us -> none  [the longest x1 10.2 us: delta_block(): jnp.einsum('nihd,nihe->ndhe', key_tail, corrected, precision=highest)]
    psum x1 -> x0, waiting for transfers between devices: 44 us -> none  [body(): lax.psum(up_part.astype(jnp.bfloat16), 'kv').astype(jnp.float32)]
    all_gather x3 -> x0, blocking collectives: 36.8 us -> none  [the longest x1 14.8 us: body(): lax.all_gather(flat_rows, 'tp', axis=1, tiled=True).astype(jnp.float32)]
    psum x2 -> x0, blocking collectives: 24.4 us -> none  [the longest x1 12.2 us: body(): squares_all = lax.psum(squares_in, 'kv')]
    unnamed x10 -> x0, waiting for transfers between devices: 22.8 us -> none
    unnamed x42 -> x8, local copies, waits for them, and re-layouts: 15 us -> 18.5 us
  transfers between devices with their start and end apart: 8 -> 0, of which waited for: 8 -> 0; matrix products, arithmetic and copies ran while one was open for 9% -> 0% of each run, Pallas kernels for 0% -> 0%
where the time goes in v1:
time: 87.9 us; the launch traced here: 87.6 us
  Pallas kernels  68.4 us (78%)
  local copies, waits for them, and re-layouts  18.5 us (21%)
    pallas_call x1, Pallas kernels, fused_layer(): pl.pallas_call(lambda *refs: layer_kernel(dims, *refs), out_shape=(jax.Sh...  68.4 us
    unnamed x8, local copies, waits for them, and re-layouts  18.5 us

profile of v1, /device:TPU:0, one launch (start us, length us, event | category | flops | bytes accessed | tf_op | source)
XLA Modules:
  0.0 87.6 jit_solution(13544026362326059969)
XLA Ops:
  0.6 2.3 %copy.19.refs_7_ = bf16[4096,32]{1,0:T(8,128)(2,1)} copy(bf16[4096,32]{0,1:T(8,128)(2,1)} %param.24) | data formatting | bytes 524288 | tf_op args[7]
  2.9 2.3 %copy.20.refs_8_ = bf16[4096,32]{1,0:T(8,128)(2,1)} copy(bf16[4096,32]{0,1:T(8,128)(2,1)} %param.25) | data formatting | bytes 524288 | tf_op args[8]
  5.2 0.0 copy-start
  5.2 4.7 %copy.21.refs_14_ = bf16[512,2752]{1,0:T(8,128)(2,1)} copy(bf16[512,2752]{0,1:T(8,128)(2,1)} %param.31) | data formatting | bytes 5636096 | tf_op args[14]
  9.9 0.0 copy-done
  9.9 3.0 %copy.22.refs_15_ = bf16[512,2752]{1,0:T(8,128)(2,1)} copy(bf16[512,2752]{0,1:T(8,128)(2,1)S(1)} %copy-done) | data formatting | bytes 5636096 | tf_op args[15]
  12.9 68.4 %shard_map.176 = (bf16[256,128]{1,0:T(8,128)(2,1)}, f32[8,128,1024]{2,1,0:T(8,128)}) custom-call(bf16[256,128]{1,0:T(8,128)(2,1)} %bitcast.8, s32[1,64]{1,0:T(1,128)} %bitcast.12, f32[8,128,1024]{2,1,0:T(8,128)} %refs_2_.1, f32[1,512]{1,0:T(1,128)} %bitcast.10, bf16[512,1024]{1,0:T(8,128)(2,1)} %refs_4_.1, bf16[512,1024]{1,0:T(8,128)(2,1)} %refs_5_.1, ...), custom_call_target="tpu_custom_call" | custom-call | tf_op jit(solution)/shard_map/pallas_call | solution.py:706
  81.3 1.5 %copy.25 = bf16[64,4,128]{2,1,0:T(4,128)(2,1)} copy(bf16[64,4,128]{2,1,0:T(4,128)(2,1)} %bitcast.9) | data formatting | bytes 131072
  82.8 4.8 %copy.26 = f32[8,128,1024]{2,1,0:T(8,128)} copy(f32[8,128,1024]{2,1,0:T(8,128)} %get-tuple-element.9) | data formatting | bytes 8388608
Async XLA Ops:
  5.2 4.7 %copy-start = (bf16[512,2752]{0,1:T(8,128)(2,1)S(1)}, bf16[512,2752]{0,1:T(8,128)(2,1)}, u32[]{:S(2)}) copy-start(bf16[512,2752]{0,1:T(8,128)(2,1)} %param.32) | copy-start | bytes 8454148

commit v2 on v1

--- a/solution.py
+++ b/solution.py
@@ -196,6 +196,10 @@
 
 def dot(a, b):
     return jnp.dot(a, b, preferred_element_type=F32)
+
+
+def dot_t(a, b):
+    return lax.dot_general(a, b, (((1,), (1,)), ((), ())), preferred_element_type=F32)
 
 
 def dot_exact(a, b):
@@ -260,6 +264,10 @@
     hid_all,
     down_part,
     down_recv,
+    placed_ref,
+    square_ref,
+    normed_ref,
+    side_ref,
     load_sem,
     store_sem,
     tp_send,
@@ -271,7 +279,7 @@
     fwd_send,
     fwd_recv,
 ):
-    n_kv, n_tp, batch, span, seqs, heads, size, width, ff, rows, unit = dims
+    n_kv, n_tp, batch, span, seqs, heads, size, width, ff, rows, packs, unit = dims
     chips = n_kv // 2
     kv = lax.axis_index("kv")
     tp = lax.axis_index("tp")
@@ -294,10 +302,10 @@
         pltpu.make_async_copy(wk_hbm, w_qkv.at[1], load_sem.at[1]),
         pltpu.make_async_copy(wv_hbm, w_qkv.at[2], load_sem.at[2]),
         pltpu.make_async_copy(
-            wb_hbm.at[pl.ds(pl.multiple_of(kv * width, width), width), :], w_beta, load_sem.at[3]
+            wb_hbm.at[:, pl.ds(pl.multiple_of(kv * width, width), width)], w_beta, load_sem.at[3]
         ),
         pltpu.make_async_copy(
-            wa_hbm.at[pl.ds(pl.multiple_of(kv * width, width), width), :], w_alpha, load_sem.at[4]
+            wa_hbm.at[:, pl.ds(pl.multiple_of(kv * width, width), width)], w_alpha, load_sem.at[4]
         ),
         pltpu.make_async_copy(state_hbm, state, load_sem.at[5]),
         pltpu.make_async_copy(wo_hbm, w_out, load_sem.at[6]),
@@ -326,7 +334,7 @@
     before = (iota((slots, slots), 0) < iota((slots, slots), 1)).astype(BF16)
     slot_row = dot(live_row.astype(BF16), before)
     slot_row = jnp.where(live_row > 0.0, slot_row, -1.0)[0:1, :]
-    picker = (iota((rows, slots), 0).astype(F32) == slot_row).astype(BF16)
+    picker = (iota((packs, slots), 0).astype(F32) == slot_row).astype(BF16)
     position = iota((slots, slots), 1) // local
     inner = lax.rem(iota((slots, slots), 1), local)
     from_slot = (
@@ -380,64 +388,105 @@
     placed = place(normed)
     square_placed = place(square_pair)
     half = chips * local
-    n_heads_all = wb_hbm.shape[1]
+    n_heads_all = wb_hbm.shape[0]
     qkv_width = 3 * vw + 128
-    for load in loads[0:5]:
-        load.wait()
-    for c in range(2):
-        here = placed[c * half : (c + 1) * half, :]
-        part = slice(c * half, (c + 1) * half)
-        for m in range(3):
-            qkv_part[part, m * vw : (m + 1) * vw] = dot(here, w_qkv[m]).astype(BF16)
-        extra = jnp.concatenate(
-            [
-                dot(here, w_beta[...]),
-                dot(here, w_alpha[...]),
-                square_placed[part, :].astype(F32),
-                jnp.zeros((half, 128 - 2 * n_heads_all - 2), F32),
-            ],
-            axis=1,
-        )
-        qkv_part[part, 3 * vw : qkv_width] = extra.astype(BF16)
-
-    pair_copy = pltpu.make_async_remote_copy(
-        src_ref=qkv_part.at[pl.ds(pl.multiple_of(other * half, half), half), :],
-        dst_ref=qkv_pair,
-        send_sem=pair_send.at[0],
-        recv_sem=pair_recv.at[0],
-        device_id={"kv": partner},
-        device_id_type=MESH,
-    )
-    pair_copy.start()
-    pair_copy.wait()
-    copies = []
-    for d in range(1, chips):
-        dest = chip_at(d)
-        at = pl.ds(pl.multiple_of(dest * local, local), local)
-        mine = pl.ds(pl.multiple_of(core * half + dest * local, local), local)
-        qkv_red[d - 1] = (qkv_part[mine, :].astype(F32) + qkv_pair[at, :].astype(F32)).astype(BF16)
-        copies.append(
-            pltpu.make_async_remote_copy(
-                src_ref=qkv_red.at[d - 1],
-                dst_ref=qkv_recv.at[d - 1],
-                send_sem=chip_send.at[0, d - 1],
-                recv_sem=chip_recv.at[0, d - 1],
-                device_id={"kv": dest * 2 + core},
-                device_id_type=MESH,
-            )
-        )
-        copies[-1].start()
-    at = pl.ds(pl.multiple_of(chip * local, local), local)
-    mine = pl.ds(pl.multiple_of(core * half + chip * local, local), local)
-    total = qkv_part[mine, :].astype(F32) + qkv_pair[at, :].astype(F32)
+    first = 128 + vw
+    chunks = ((0, first), (first, first + vw), (first + vw, qkv_width))
+
+    def halves(c, size_of):
+        return pl.ds(pl.multiple_of(c * size_of, size_of), size_of)
+
+    def pair_start(index, source, dest):
+        copy = pltpu.make_async_remote_copy(
+            src_ref=source,
+            dst_ref=dest,
+            send_sem=pair_send.at[index],
+            recv_sem=pair_recv.at[index],
+            device_id={"kv": partner},
+            device_id_type=MESH,
+        )
+        copy.start()
+        return copy
+
+    def chip_start(index, d, source, dest):
+        copy = pltpu.make_async_remote_copy(
+            src_ref=source,
+            dst_ref=dest,
+            send_sem=chip_send.at[index, d - 1],
+            recv_sem=chip_recv.at[index, d - 1],
+            device_id={"kv": chip_at(d) * 2 + core},
+            device_id_type=MESH,
+        )
+        copy.start()
+        return copy
+
+    placed_ref[...] = placed
+    square_ref[...] = square_placed
+
+    def qkv_chunk(m, c):
+        part = halves(c, half)
+        here = placed_ref[part, :]
+        low, high = chunks[m]
+        if m == 0:
+            extra = jnp.concatenate(
+                [
+                    dot_t(here, w_beta[...]),
+                    dot_t(here, w_alpha[...]),
+                    square_ref[part, :].astype(F32),
+                    jnp.zeros((half, 128 - 2 * n_heads_all - 2), F32),
+                ],
+                axis=1,
+            )
+            qkv_part[part, 0:128] = extra.astype(BF16)
+            low = 128
+        qkv_part[part, low:high] = dot(here, w_qkv[(1, 0, 2)[m]]).astype(BF16)
+
+    def qkv_finish(m):
+        pair_copies[m].wait()
+        cols = slice(*chunks[m])
+        for d in range(1, chips):
+            dest = chip_at(d)
+            at = halves(dest, local)
+            mine = pl.ds(pl.multiple_of(core * half + dest * local, local), local)
+            qkv_red[d - 1, :, cols] = (
+                qkv_part[mine, cols].astype(F32) + qkv_pair[at, cols].astype(F32)
+            ).astype(BF16)
+            qkv_far[m].append(
+                chip_start(m, d, qkv_red.at[d - 1, :, cols], qkv_recv.at[d - 1, :, cols])
+            )
+
+    pair_copies = []
+    qkv_far = [[], [], []]
+    for m in range(3):
+        loads[(1, 0, 2)[m]].wait()
+        if m == 0:
+            loads[3].wait()
+            loads[4].wait()
+        qkv_chunk(m, other)
+        cols = slice(*chunks[m])
+        pair_copies.append(
+            pair_start(m, qkv_part.at[halves(other, half), cols], qkv_pair.at[:, cols])
+        )
+        qkv_chunk(m, core)
+        if m > 0:
+            qkv_finish(m - 1)
+    qkv_finish(2)
 
     loads[5].wait()
     state_low = state[...].reshape(seqs * size, vw).astype(BF16)
-    exchange_wait(copies)
-    for d in range(1, chips):
-        total = total + qkv_recv[d - 1].astype(F32)
-
-    extra = total[:, 3 * vw : qkv_width]
+
+    def own_sum(m):
+        exchange_wait(qkv_far[m])
+        cols = slice(*chunks[m])
+        at = halves(chip, local)
+        mine = pl.ds(pl.multiple_of(core * half + chip * local, local), local)
+        total = qkv_part[mine, cols].astype(F32) + qkv_pair[at, cols].astype(F32)
+        for d in range(1, chips):
+            total = total + qkv_recv[d - 1, :, cols].astype(F32)
+        return total
+
+    extra_keys = own_sum(0)
+    extra = extra_keys[:, 0:128]
     lane = iota((local, 128), 1)
     sq_lane = (lane == 2 * n_heads_all) | (lane == 2 * n_heads_all + 1)
     sq_own = jnp.sum(jnp.where(sq_lane, extra, 0.0), axis=1, keepdims=True)
@@ -459,11 +508,10 @@
     softplus = jnp.maximum(pre, 0.0) + jnp.log(1.0 + jnp.exp(-jnp.abs(pre)))
     log_decay = jnp.where(live, -rate * softplus, 0.0)
 
-    q_raw = total[:, 0:vw] * row_scale
-    k_raw = total[:, vw : 2 * vw] * row_scale
-    values = total[:, 2 * vw : 3 * vw] * row_scale
+    k_raw = extra_keys[:, 128:] * row_scale
+    keys = k_raw * lax.rsqrt(head_sum(k_raw * k_raw, heads, size) + EPSILON)
+    q_raw = own_sum(1) * row_scale
     queries = q_raw * lax.rsqrt(head_sum(q_raw * q_raw, heads, size) + EPSILON) * size ** (-0.5)
-    keys = k_raw * lax.rsqrt(head_sum(k_raw * k_raw, heads, size) + EPSILON)
 
     def token(x, t):
         return x[t * seqs : (t + 1) * seqs, :]
@@ -484,6 +532,7 @@
         both = jnp.concatenate([keys[:, cols], queries[:, cols]], axis=0)
         products.append(dot(blocked(both), state_low[:, cols]))
     products = jnp.concatenate(products, axis=1)
+    values = own_sum(2) * row_scale
     updates, attended = [], []
     for t in range(span):
         grown = jnp.exp(cumulative[t])
@@ -519,8 +568,8 @@
             pltpu.make_async_remote_copy(
                 src_ref=buffer.at[spot],
                 dst_ref=buffer.at[spot],
-                send_sem=chip_send.at[1 + 2 * phase, d - 1],
-                recv_sem=chip_recv.at[1 + 2 * phase, d - 1],
+                send_sem=chip_send.at[7 + phase, d - 1],
+                recv_sem=chip_recv.at[7 + phase, d - 1],
                 device_id={"kv": chip_at(d) * 2 + core},
                 device_id_type=MESH,
             )
@@ -603,48 +652,65 @@
     middle_rows = jnp.concatenate([mid_all[j] for j in range(n_tp)], axis=1).astype(F32)
     squares = jnp.sum(middle_rows * middle_rows, axis=1, keepdims=True)
     normed_mid = (middle_rows * mix_gain_ref[...]).astype(BF16)
+    ff_pad = gu_part.shape[2]
+    pad = ff_pad - ff
+    empty = rows - packs
+    if empty:
+        normed_mid = jnp.concatenate([normed_mid, jnp.zeros((empty, width), BF16)], axis=0)
+        squares = jnp.concatenate([squares, jnp.zeros((empty, 1), F32)], axis=0)
     square_high, square_low = high_low(squares)
-    pad = gu_part.shape[2] - ff
-    side = jnp.concatenate([square_high, square_low, jnp.zeros((rows, pad - 2), F32)], axis=1)
     half = chips * unit
-    copies = []
-    for m in range(2):
-        loads[7 + m].wait()
-        gu_part[m, :, 0:ff] = dot(normed_mid, (w_gate, w_up)[m][...]).astype(BF16)
-        gu_part[m, :, ff:] = (side if m == 0 else jnp.zeros((rows, pad), F32)).astype(BF16)
-        copies.append(
-            pltpu.make_async_remote_copy(
-                src_ref=gu_part.at[m, pl.ds(pl.multiple_of(other * half, half), half), :],
-                dst_ref=gu_pair.at[m],
-                send_sem=pair_send.at[1 + m],
-                recv_sem=pair_recv.at[1 + m],
-                device_id={"kv": partner},
-                device_id_type=MESH,
-            )
-        )
-        copies[-1].start()
-    far = []
-    for m in range(2):
-        copies[m].wait()
+    normed_ref[...] = normed_mid
+    side_ref[...] = jnp.concatenate(
+        [square_high, square_low, jnp.zeros((rows, pad - 2), F32)], axis=1
+    )
+    middle_col = ff_pad // 256 * 128
+    gu_chunks = [(m, low, high) for low, high in ((0, middle_col), (middle_col, ff_pad)) for m in range(2)]
+
+    def gu_chunk(index, c):
+        m, low, high = gu_chunks[index]
+        part = halves(c, half)
+        stop = min(high, ff)
+        weights = (w_gate, w_up)[m]
+        gu_part[m, part, low:stop] = dot_t(normed_ref[part, :], weights[low:stop, :]).astype(BF16)
+        if high > ff:
+            side = side_ref[part, :] if m == 0 else jnp.zeros((half, pad), F32)
+            gu_part[m, part, ff:high] = side.astype(BF16)
+
+    def gu_finish(index):
+        gu_pairs[index].wait()
+        m, low, high = gu_chunks[index]
+        cols = slice(low, high)
         for d in range(1, chips):
             dest = chip_at(d)
-            at = pl.ds(pl.multiple_of(dest * unit, unit), unit)
+            at = halves(dest, unit)
             mine = pl.ds(pl.multiple_of(core * half + dest * unit, unit), unit)
-            gu_red[m, d - 1] = (
-                gu_part[m, mine, :].astype(F32) + gu_pair[m, at, :].astype(F32)
+            gu_red[m, d - 1, :, cols] = (
+                gu_part[m, mine, cols].astype(F32) + gu_pair[m, at, cols].astype(F32)
             ).astype(BF16)
             far.append(
-                pltpu.make_async_remote_copy(
-                    src_ref=gu_red.at[m, d - 1],
-                    dst_ref=gu_recv.at[m, d - 1],
-                    send_sem=chip_send.at[2 if m == 0 else 4, d - 1],
-                    recv_sem=chip_recv.at[2 if m == 0 else 4, d - 1],
-                    device_id={"kv": dest * 2 + core},
-                    device_id_type=MESH,
+                chip_start(
+                    3 + index, d, gu_red.at[m, d - 1, :, cols], gu_recv.at[m, d - 1, :, cols]
                 )
             )
-            far[-1].start()
-    at = pl.ds(pl.multiple_of(chip * unit, unit), unit)
+
+    gu_pairs, far = [], []
+    loads[7].wait()
+    loads[8].wait()
+    for index, (m, low, high) in enumerate(gu_chunks):
+        gu_chunk(index, other)
+        gu_pairs.append(
+            pair_start(
+                3 + index,
+                gu_part.at[m, halves(other, half), slice(low, high)],
+                gu_pair.at[m, :, slice(low, high)],
+            )
+        )
+        gu_chunk(index, core)
+        if index > 0:
+            gu_finish(index - 1)
+    gu_finish(len(gu_chunks) - 1)
+    at = halves(chip, unit)
     mine = pl.ds(pl.multiple_of(core * half + chip * unit, unit), unit)
     sums = []
     for m in range(2):
@@ -665,7 +731,7 @@
     own, far = kv_gather_start(1, hid_all)
     kv_gather_finish(1, hid_all, own, far)
     loads[9].wait()
-    hidden_all = hid_all[...].reshape(rows, hid_all.shape[2])[:, 0:ff]
+    hidden_all = hid_all[...].reshape(rows, hid_all.shape[2])[0:packs, 0:ff]
     part = dot(hidden_all, w_down[...])
     result = (middle.astype(F32) + tp_scatter(3, part, down_part, down_recv)).astype(BF16)
     mixed_ref[...] = lax.dot_general(
@@ -685,16 +751,19 @@
     pack = min(batch * 7 // 4, batch * span)
     unit = (pack + n_kv - 1) // n_kv
     unit = (unit + 15) // 16 * 16
+    packs = (pack + 15) // 16 * 16
     rows = unit * n_kv
     local = seqs * span
     chips = n_kv // 2
     ff_pad = (ff + 2 + 127) // 128 * 128
     qkv_width = 3 * vw + 128
-    dims = (n_kv, n_tp, batch, span, seqs, heads, size, width, ff, rows, unit)
+    dims = (n_kv, n_tp, batch, span, seqs, heads, size, width, ff, rows, packs, unit)
     operands = list(args)
     operands[0] = tokens.reshape(batch * span, own_cols)
     for at in (1, 3, 9, 10, 11, 13):
         operands[at] = operands[at].reshape(1, -1)
+    for at in (7, 8, 14, 15):
+        operands[at] = operands[at].T
     in_vmem = pl.BlockSpec(memory_space=pltpu.VMEM)
     in_hbm = pl.BlockSpec(memory_space=pl.ANY)
     vmem_args = (0, 1, 3, 9, 10, 11, 13)
@@ -714,36 +783,40 @@
         scratch_shapes=[
             pltpu.VMEM(state.shape, F32),
             buf(3, width, vw),
-            buf(*(width, w_beta.shape[1])),
-            buf(*(width, w_beta.shape[1])),
+            buf(w_beta.shape[1], width),
+            buf(w_beta.shape[1], width),
             buf(*w_out.shape),
-            buf(*w_gate.shape),
-            buf(*w_gate.shape),
+            buf(ff, width),
+            buf(ff, width),
             buf(ff, w_out.shape[1]),
-            buf(n_tp, rows, own_cols),
+            buf(n_tp, packs, own_cols),
             buf(n_kv * local, qkv_width),
             buf(chips * local, qkv_width),
             buf(chips - 1, local, qkv_width),
             buf(chips - 1, local, qkv_width),
             buf(n_kv, local, vw),
-            buf(n_tp, rows, own_cols),
-            buf(n_tp - 1, rows, own_cols),
-            buf(n_tp, rows, own_cols),
+            buf(n_tp, packs, own_cols),
+            buf(n_tp - 1, packs, own_cols),
+            buf(n_tp, packs, own_cols),
             buf(2, rows, ff_pad),
             buf(2, chips * unit, ff_pad),
             buf(2, chips - 1, unit, ff_pad),
             buf(2, chips - 1, unit, ff_pad),
             buf(n_kv, unit, ff_pad),
-            buf(n_tp, rows, own_cols),
-            buf(n_tp - 1, rows, own_cols),
+            buf(n_tp, packs, own_cols),
+            buf(n_tp - 1, packs, own_cols),
+            buf(n_kv * local, width),
+            buf(n_kv * local, 2),
+            buf(rows, width),
+            pltpu.VMEM((rows, ff_pad - ff), F32),
             dma((10,)),
             dma((1,)),
             dma((4, n_tp - 1)),
             dma((4, n_tp - 1)),
-            dma((3,)),
-            dma((3,)),
-            dma((5, chips - 1)),
-            dma((5, chips - 1)),
+            dma((7,)),
+            dma((7,)),
+            dma((9, chips - 1)),
+            dma((9, chips - 1)),
             dma((2, chips)),
             dma((2, chips)),
         ],

time: 87.9 us -> 71.8 us (0.82)
  local copies, waits for them, and re-layouts: 18.5 us -> 6.28 us
  Pallas kernels: 68.4 us -> 64.6 us
    unnamed x8 -> x2, local copies, waits for them, and re-layouts: 18.5 us -> 6.28 us
    pallas_call x1, Pallas kernels: 68.4 us -> 64.6 us  [fused_layer(): pl.pallas_call(lambda *refs: layer_kernel(dims, *refs), out_shape=(jax.Sh...]
where the time goes in v2:
time: 71.8 us; the launch traced here: 71.5 us
  Pallas kernels  64.6 us (90%)
  local copies, waits for them, and re-layouts  6.28 us (9%)
    pallas_call x1, Pallas kernels, fused_layer(): pl.pallas_call(lambda *refs: layer_kernel(dims, *refs), out_shape=(jax.Sh...  64.6 us
    unnamed x2, local copies, waits for them, and re-layouts  6.28 us

profile of v2, /device:TPU:0, one launch (start us, length us, event | category | flops | bytes accessed | tf_op | source)
XLA Modules:
  0.0 71.5 jit_solution(12939045519447339227)
XLA Ops:
  0.6 64.6 %shard_map.176 = (bf16[256,128]{1,0:T(8,128)(2,1)}, f32[8,128,1024]{2,1,0:T(8,128)}) custom-call(bf16[256,128]{1,0:T(8,128)(2,1)} %bitcast.16, s32[1,64]{1,0:T(1,128)} %bitcast.20, f32[8,128,1024]{2,1,0:T(8,128)} %refs_2_.1, f32[1,512]{1,0:T(1,128)} %bitcast.18, bf16[512,1024]{1,0:T(8,128)(2,1)} %refs_4_.1, bf16[512,1024]{1,0:T(8,128)(2,1)} %refs_5_.1, ...), custom_call_target="tpu_custom_call" | custom-call | tf_op jit(solution)/shard_map/pallas_call | solution.py:775
  65.2 1.5 %copy.21 = bf16[64,4,128]{2,1,0:T(4,128)(2,1)} copy(bf16[64,4,128]{2,1,0:T(4,128)(2,1)} %bitcast.17) | data formatting | bytes 131072
  66.7 4.8 %copy.22 = f32[8,128,1024]{2,1,0:T(8,128)} copy(f32[8,128,1024]{2,1,0:T(8,128)} %get-tuple-element.9) | data formatting | bytes 8388608

commit v3 on v2

--- a/solution.py
+++ b/solution.py
@@ -261,7 +261,8 @@
     gu_pair,
     gu_red,
     gu_recv,
-    hid_all,
+    hid_first,
+    hid_second,
     down_part,
     down_recv,
     placed_ref,
@@ -568,8 +569,8 @@
             pltpu.make_async_remote_copy(
                 src_ref=buffer.at[spot],
                 dst_ref=buffer.at[spot],
-                send_sem=chip_send.at[7 + phase, d - 1],
-                recv_sem=chip_recv.at[7 + phase, d - 1],
+                send_sem=chip_send.at[8 + phase, d - 1],
+                recv_sem=chip_recv.at[8 + phase, d - 1],
                 device_id={"kv": chip_at(d) * 2 + core},
                 device_id_type=MESH,
             )
@@ -631,24 +632,46 @@
     part = dot(packed, w_out[...])
     own_cols = tokens_ref.shape[1]
 
-    def tp_scatter(phase, part, part_ref, recv_ref):
+    def tp_scatter_start(phase, part, part_ref, recv_ref, group):
         for j in range(n_tp):
-            part_ref[j] = part[:, j * own_cols : (j + 1) * own_cols].astype(BF16)
+            part_ref[j, group, :] = part[group, j * own_cols : (j + 1) * own_cols].astype(BF16)
         copies = tp_copies(
-            phase, lambda peer, d: part_ref.at[peer], lambda peer, d: recv_ref.at[d - 1]
+            phase,
+            lambda peer, d: part_ref.at[peer, group, :],
+            lambda peer, d: recv_ref.at[d - 1, group, :],
         )
         exchange_start(copies)
+        return copies
+
+    def tp_scatter_finish(copies, part_ref, recv_ref, group):
         exchange_wait(copies)
-        total = part_ref[tp].astype(F32)
+        total = part_ref[tp, group, :].astype(F32)
         for d in range(1, n_tp):
-            total = total + recv_ref[d - 1].astype(F32)
+            total = total + recv_ref[d - 1, group, :].astype(F32)
         return total
 
-    middle = (own_tokens + tp_scatter(1, part, attn_part, attn_recv)).astype(BF16)
-    mid_all[tp] = middle
-    copies = tp_copies(2, lambda peer, d: mid_all.at[tp], lambda peer, d: mid_all.at[tp])
-    exchange_start(copies)
-    exchange_wait(copies)
+    cut = packs // 32 * 16
+    groups = (slice(0, cut), slice(cut, packs))
+    scatters = [
+        tp_scatter_start((1, 4)[i], part, attn_part, attn_recv, group)
+        for i, group in enumerate(groups)
+    ]
+    gathers = []
+    for i, group in enumerate(groups):
+        middle = (
+            own_tokens[group, :] + tp_scatter_finish(scatters[i], attn_part, attn_recv, group)
+        ).astype(BF16)
+        mid_all[tp, group, :] = middle
+        gathers.append(
+            tp_copies(
+                (2, 5)[i],
+                lambda peer, d: mid_all.at[tp, group, :],
+                lambda peer, d: mid_all.at[tp, group, :],
+            )
+        )
+        exchange_start(gathers[-1])
+    for copies in gathers:
+        exchange_wait(copies)
     middle_rows = jnp.concatenate([mid_all[j] for j in range(n_tp)], axis=1).astype(F32)
     squares = jnp.sum(middle_rows * middle_rows, axis=1, keepdims=True)
     normed_mid = (middle_rows * mix_gain_ref[...]).astype(BF16)
@@ -665,14 +688,24 @@
         [square_high, square_low, jnp.zeros((rows, pad - 2), F32)], axis=1
     )
     middle_col = ff_pad // 256 * 128
-    gu_chunks = [(m, low, high) for low, high in ((0, middle_col), (middle_col, ff_pad)) for m in range(2)]
+    last_col = ff // 128 * 128
+    gu_chunks = (
+        (0, last_col, ff_pad),
+        (0, 0, middle_col),
+        (1, 0, middle_col),
+        (0, middle_col, last_col),
+        (1, middle_col, ff_pad),
+    )
 
     def gu_chunk(index, c):
         m, low, high = gu_chunks[index]
         part = halves(c, half)
         stop = min(high, ff)
         weights = (w_gate, w_up)[m]
-        gu_part[m, part, low:stop] = dot_t(normed_ref[part, :], weights[low:stop, :]).astype(BF16)
+        if stop > low:
+            gu_part[m, part, low:stop] = dot_t(normed_ref[part, :], weights[low:stop, :]).astype(
+                BF16
+            )
         if high > ff:
             side = side_ref[part, :] if m == 0 else jnp.zeros((half, pad), F32)
             gu_part[m, part, ff:high] = side.astype(BF16)
@@ -688,13 +721,13 @@
             gu_red[m, d - 1, :, cols] = (
                 gu_part[m, mine, cols].astype(F32) + gu_pair[m, at, cols].astype(F32)
             ).astype(BF16)
-            far.append(
+            gu_far[index].append(
                 chip_start(
                     3 + index, d, gu_red.at[m, d - 1, :, cols], gu_recv.at[m, d - 1, :, cols]
                 )
             )
 
-    gu_pairs, far = [], []
+    gu_pairs, gu_far = [], [[] for _ in gu_chunks]
     loads[7].wait()
     loads[8].wait()
     for index, (m, low, high) in enumerate(gu_chunks):
@@ -712,28 +745,45 @@
     gu_finish(len(gu_chunks) - 1)
     at = halves(chip, unit)
     mine = pl.ds(pl.multiple_of(core * half + chip * unit, unit), unit)
-    sums = []
-    for m in range(2):
-        sums.append(gu_part[m, mine, :].astype(F32) + gu_pair[m, at, :].astype(F32))
-    exchange_wait(far)
-    for m in range(2):
+
+    def gu_sum(index):
+        exchange_wait(gu_far[index])
+        m, low, high = gu_chunks[index]
+        cols = slice(low, high)
+        total = gu_part[m, mine, cols].astype(F32) + gu_pair[m, at, cols].astype(F32)
         for d in range(1, chips):
-            sums[m] = sums[m] + gu_recv[m, d - 1].astype(F32)
-    gate, up = sums
-    lane = iota(gate.shape, 1)
+            total = total + gu_recv[m, d - 1, :, cols].astype(F32)
+        return total
+
+    spot = core * chips + chip
+    gate_last = gu_sum(0)
+    lane = iota(gate_last.shape, 1) + last_col
     sq_mid = jnp.sum(
-        jnp.where((lane == ff) | (lane == ff + 1), gate, 0.0), axis=1, keepdims=True
+        jnp.where((lane == ff) | (lane == ff + 1), gate_last, 0.0), axis=1, keepdims=True
     )
     mid_scale = lax.rsqrt(sq_mid / D + EPSILON)
-    gate = jnp.where(lane < ff, gate * mid_scale, 0.0)
-    hidden = gate / (1.0 + jnp.exp(-gate)) * (up * mid_scale)
-    hid_all[core * chips + chip] = hidden.astype(BF16)
-    own, far = kv_gather_start(1, hid_all)
-    kv_gather_finish(1, hid_all, own, far)
+    gate_last = jnp.where(lane < ff, gate_last, 0.0)
+
+    def hidden_of(gate, up):
+        gate = gate * mid_scale
+        return (gate / (1.0 + jnp.exp(-gate)) * (up * mid_scale)).astype(BF16)
+
+    hid_first[spot] = hidden_of(gu_sum(1), gu_sum(2))
+    own_first, far_first = kv_gather_start(1, hid_first)
+    gate = jnp.concatenate([gu_sum(3), gate_last], axis=1)
+    hid_second[spot] = hidden_of(gate, gu_sum(4))
+    own_second, far_second = kv_gather_start(2, hid_second)
+    kv_gather_finish(1, hid_first, own_first, far_first)
     loads[9].wait()
-    hidden_all = hid_all[...].reshape(rows, hid_all.shape[2])[0:packs, 0:ff]
-    part = dot(hidden_all, w_down[...])
-    result = (middle.astype(F32) + tp_scatter(3, part, down_part, down_recv)).astype(BF16)
+    hidden_all = hid_first[...].reshape(rows, middle_col)[0:packs, :]
+    part = dot(hidden_all, w_down[0:middle_col, :])
+    kv_gather_finish(2, hid_second, own_second, far_second)
+    hidden_all = hid_second[...].reshape(rows, ff_pad - middle_col)[0:packs, 0 : ff - middle_col]
+    part = part + dot(hidden_all, w_down[middle_col:ff, :])
+    every = slice(0, packs)
+    copies = tp_scatter_start(3, part, down_part, down_recv, every)
+    down = tp_scatter_finish(copies, down_part, down_recv, every)
+    result = (mid_all[tp].astype(F32) + down).astype(BF16)
     mixed_ref[...] = lax.dot_general(
         picker, result, (((0,), (0,)), ((), ())), preferred_element_type=F32
     ).astype(BF16)
@@ -802,7 +852,8 @@
             buf(2, chips * unit, ff_pad),
             buf(2, chips - 1, unit, ff_pad),
             buf(2, chips - 1, unit, ff_pad),
-            buf(n_kv, unit, ff_pad),
+            buf(n_kv, unit, ff_pad // 256 * 128),
+            buf(n_kv, unit, ff_pad - ff_pad // 256 * 128),
             buf(n_tp, packs, own_cols),
             buf(n_tp - 1, packs, own_cols),
             buf(n_kv * local, width),
@@ -811,14 +862,14 @@
             pltpu.VMEM((rows, ff_pad - ff), F32),
             dma((10,)),
             dma((1,)),
-            dma((4, n_tp - 1)),
-            dma((4, n_tp - 1)),
-            dma((7,)),
-            dma((7,)),
-            dma((9, chips - 1)),
-            dma((9, chips - 1)),
-            dma((2, chips)),
-            dma((2, chips)),
+            dma((6, n_tp - 1)),
+            dma((6, n_tp - 1)),
+            dma((8,)),
+            dma((8,)),
+            dma((11, chips - 1)),
+            dma((11, chips - 1)),
+            dma((3, chips)),
+            dma((3, chips)),
         ],
         compiler_params=pltpu.CompilerParams(
             collective_id=0, has_side_effects=True, vmem_limit_bytes=60 * 1024 * 1024

time: 71.8 us -> 71.7 us (level)
  no operation moved by 1% of the time
where the time goes in v3:
time: 71.7 us; the launch traced here: 71.4 us
  Pallas kernels  64.5 us (90%)
  local copies, waits for them, and re-layouts  6.28 us (9%)
    pallas_call x1, Pallas kernels, fused_layer(): pl.pallas_call(lambda *refs: layer_kernel(dims, *refs), out_shape=(jax.Sh...  64.5 us
    unnamed x2, local copies, waits for them, and re-layouts  6.28 us

profile of v3, /device:TPU:0, one launch (start us, length us, event | category | flops | bytes accessed | tf_op | source)
XLA Modules:
  0.0 71.4 jit_solution(14987259532290764300)
XLA Ops:
  0.6 64.5 %shard_map.176 = (bf16[256,128]{1,0:T(8,128)(2,1)}, f32[8,128,1024]{2,1,0:T(8,128)}) custom-call(bf16[256,128]{1,0:T(8,128)(2,1)} %bitcast.16, s32[1,64]{1,0:T(1,128)} %bitcast.20, f32[8,128,1024]{2,1,0:T(8,128)} %refs_2_.1, f32[1,512]{1,0:T(1,128)} %bitcast.18, bf16[512,1024]{1,0:T(8,128)(2,1)} %refs_4_.1, bf16[512,1024]{1,0:T(8,128)(2,1)} %refs_5_.1, ...), custom_call_target="tpu_custom_call" | custom-call | tf_op jit(solution)/shard_map/pallas_call | solution.py:825
  65.2 1.5 %copy.21 = bf16[64,4,128]{2,1,0:T(4,128)(2,1)} copy(bf16[64,4,128]{2,1,0:T(4,128)(2,1)} %bitcast.17) | data formatting | bytes 131072
  66.7 4.8 %copy.22 = f32[8,128,1024]{2,1,0:T(8,128)} copy(f32[8,128,1024]{2,1,0:T(8,128)} %get-tuple-element.9) | data formatting | bytes 8388608

commit v4 on v3

--- a/solution.py
+++ b/solution.py
@@ -875,7 +875,36 @@
             collective_id=0, has_side_effects=True, vmem_limit_bytes=60 * 1024 * 1024
         ),
     )(*operands)
-    return mixed.reshape(tokens.shape), new_state
+    count = state.shape[0]
+    return pl.pallas_call(
+        finish_kernel,
+        out_shape=(
+            jax.ShapeDtypeStruct(tokens.shape, BF16),
+            jax.ShapeDtypeStruct(state.shape, F32),
+        ),
+        in_specs=[in_vmem, in_hbm],
+        out_specs=(in_vmem, in_hbm),
+        scratch_shapes=[pltpu.VMEM(state.shape, F32), dma((count,)), dma((count,))],
+        compiler_params=pltpu.CompilerParams(vmem_limit_bytes=60 * 1024 * 1024),
+    )(mixed, new_state)
+
+
+def finish_kernel(mixed_ref, state_hbm, mixed_out, state_out, buffer, read_sem, write_sem):
+    count = buffer.shape[0]
+    reads = [
+        pltpu.make_async_copy(state_hbm.at[n], buffer.at[n], read_sem.at[n]) for n in range(count)
+    ]
+    writes = [
+        pltpu.make_async_copy(buffer.at[n], state_out.at[n], write_sem.at[n]) for n in range(count)
+    ]
+    for read in reads:
+        read.start()
+    mixed_out[...] = mixed_ref[...].astype(F32).reshape(mixed_out.shape).astype(BF16)
+    for read, write in zip(reads, writes):
+        read.wait()
+        write.start()
+    for write in writes:
+        write.wait()
 
 
 def layer(*args):

time: 71.7 us -> 70.4 us (0.982)
  local copies, waits for them, and re-layouts: 6.28 us -> 0 us
  Pallas kernels: 64.5 us -> 69.6 us
    unnamed x2 -> x0, local copies, waits for them, and re-layouts: 6.28 us -> none
    pallas_call x0 -> x1, Pallas kernels: none -> 5.05 us  [fused_layer(): pl.pallas_call(finish_kernel, out_shape=(jax.ShapeDtypeStruct(tokens.shap...]
where the time goes in v4:
time: 70.4 us; the launch traced here: 70.2 us
  Pallas kernels  69.6 us (99%)
    pallas_call x1, Pallas kernels, fused_layer(): pl.pallas_call(lambda *refs: layer_kernel(dims, *refs), out_shape=(jax.Sh...  64.5 us
    pallas_call x1, Pallas kernels, fused_layer(): pl.pallas_call(finish_kernel, out_shape=(jax.ShapeDtypeStruct(tokens.shap...  5.05 us

profile of v4, /device:TPU:0, one launch (start us, length us, event | category | flops | bytes accessed | tf_op | source)
XLA Modules:
  0.0 70.2 jit_solution(10124595048480249610)
XLA Ops:
  0.6 64.5 %shard_map.176 = (bf16[256,128]{1,0:T(8,128)(2,1)}, f32[8,128,1024]{2,1,0:T(8,128)}) custom-call(bf16[256,128]{1,0:T(8,128)(2,1)} %bitcast.15, s32[1,64]{1,0:T(1,128)} %bitcast.18, f32[8,128,1024]{2,1,0:T(8,128)} %refs_2_.1, f32[1,512]{1,0:T(1,128)} %bitcast.16, bf16[512,1024]{1,0:T(8,128)(2,1)} %refs_4_.1, bf16[512,1024]{1,0:T(8,128)(2,1)} %refs_5_.1, ...), custom_call_target="tpu_custom_call" | custom-call | tf_op jit(solution)/shard_map/pallas_call | solution.py:825
  65.2 5.0 %shard_map.177 = (bf16[64,4,128]{2,1,0:T(4,128)(2,1)}, f32[8,128,1024]{2,1,0:T(8,128)}) custom-call(bf16[256,128]{1,0:T(8,128)(2,1)} %get-tuple-element.4.mixed_ref, f32[8,128,1024]{2,1,0:T(8,128)} %get-tuple-element.5.state_hbm), custom_call_target="tpu_custom_call" | custom-call | tf_op jit(solution)/shard_map/pallas_call | solution.py:879
